TPU v7x, 32 devices: a whole 2x2x4 slice. The times are simulated.
32 devices in a mesh: sp: 8 (over z, y), tp: 4 (over x, core).
Axes of the slice: x: 2, y: 2, z: 4, core: 2. Of those that a mesh axis runs over, the one named last changes fastest.
Arguments:
- glu_value: bfloat16 [4096, 2048], P('sp', 'tp'), may hold values from -640 to 640
- glu_gate: bfloat16 [4096, 2048], P('sp', 'tp'), may hold values from -9 to 9
- conv_kernel: float32 [31, 2048], P(None, 'tp'), may hold values from -1 to 1
- norm_gain: float32 [2048], P('tp'), may hold values from 0.1 to 1.9
- mix_weight: bfloat16 [2048, 2048], P('tp'), may hold values from -0.125 to 0.125
- residual: bfloat16 [4096, 2048], P(('sp', 'tp')), may hold values from -6 to 6
- resid_gain: float32 [2048], replicated, may hold values from 0.1 to 1.9
- expert_ids: int32 [4096, 2], P(('sp', 'tp')), may hold values from 0 to 7, all different within a row; in each aligned block of 128 rows (0 to 127, 128 to 255, ...) at most 64 rows name the same one
- route_weight: float32 [4096, 2], P(('sp', 'tp')), may hold values from 0.05 to 0.5
- w_gate: bfloat16 [8, 2048, 2048], P('sp', None, 'tp'), may hold values from -0.5 to 0.5
- w_up: bfloat16 [8, 2048, 2048], P('sp', None, 'tp'), may hold values from -0.5 to 0.5
- w_down: bfloat16 [8, 2048, 2048], P('sp', 'tp'), may hold values from -0.03125 to 0.03125
- out_gain: float32 [2048], replicated, may hold values from 0.1 to 1.9
Outputs:
- blended: bfloat16 [4096, 2048], P(('sp', 'tp'))
Inputs may be any that keep to these rules, and one draw needn't show every extreme that they name: `expert_ids`: in each aligned block of 128 rows (the rows of one device) no expert is named by more than 64 rows, a bound that some block reaches.
All inputs are finite; a program needn't handle non-finite values.
Results may differ from a plain program's by a relative error of at most 0.015.
Values may be sent and summed in bfloat16 or wider, within the bound.
A program may use at most 128 MiB of HBM per device.

v0:
```python
import functools

import jax
import jax.numpy as jnp
from jax import lax
from jax.experimental import pallas as pl
from jax.experimental.pallas import tpu as pltpu
from jax.sharding import PartitionSpec as P

DC = 2048


EPSILON = 1e-05
LIMIT = 7.0
SLOPE = 1.702


def shifted(block, axis, distance):
    devices = range(lax.axis_size(axis))
    route = [(i - distance, i) for i in devices if i - distance in devices]
    return lax.ppermute(block, axis, route)


def normalize(values, gain_vector):
    centre = jnp.mean(values, axis=-1, keepdims=True)
    spread = jnp.mean(jnp.square(values - centre), axis=-1, keepdims=True)
    return (values - centre) * lax.rsqrt(spread + EPSILON) * gain_vector


def swapped(block, stride):
    route = [(i, i ^ stride) for i in range(lax.axis_size("tp"))]
    return lax.ppermute(block, "tp", route)


def slot_layout(route_ids, experts, capacity):
    row_count, top_count = route_ids.shape
    flat_ids = route_ids.reshape(row_count * top_count)
    onehot = (flat_ids[:, None] == jnp.arange(experts, dtype=jnp.int32)[None, :]).astype(jnp.int32)
    before = jnp.cumsum(onehot, axis=0) - onehot
    slot_rank = jnp.sum(before * onehot, axis=1)
    position = flat_ids * capacity + slot_rank
    return position.reshape(row_count, top_count)


MESH = pl.DeviceIdType.MESH
GROUPS = 8
ARRIVAL = (0, 1, 4, 2, 5, 3, 6, 7)
RETURN = (4, 5, 6, 7, 2, 3, 1, 0)


def flipped(index, mask):
    result = index
    bit = 1
    while bit <= mask:
        if mask & bit:
            result = result + bit - 2 * bit * lax.rem(lax.div(index, bit), 2)
        bit *= 2
    return result


def experts_kernel(
    count,
    slots,
    gate_hbm,
    up_hbm,
    down_hbm,
    out,
    rows,
    outp,
    nrecv,
    frecv,
    act,
    gate,
    up,
    down,
    weight_sem,
    local_sem,
    disp_send,
    disp_recv,
    hop_send,
    hop_recv,
    ret_send,
    ret_recv,
):
    total = slots.shape[0]
    cap = total // count
    size = total // GROUPS
    per = count // GROUPS
    me = lax.axis_index("sp")
    place = lax.axis_index("tp")
    near = flipped(place, 1)
    far = flipped(place, 2)
    hidden, width = down.shape

    loads = [
        pltpu.make_async_copy(source, target, weight_sem.at[i])
        for i, (source, target) in enumerate(((gate_hbm, gate), (up_hbm, up), (down_hbm, down)))
    ]
    for load in loads:
        load.start()

    barrier = pltpu.get_barrier_semaphore()
    for k in range(1, count):
        pl.semaphore_signal(barrier, inc=1, device_id={"sp": flipped(me, k)}, device_id_type=MESH)
    for other in (near, far):
        pl.semaphore_signal(barrier, inc=1, device_id={"tp": other}, device_id_type=MESH)
    pl.semaphore_wait(barrier, count + 1)

    def spot(g, side):
        return pl.ds((2 * ARRIVAL.index(g) + side) * size, size)

    def spot_of(k):
        return pl.ds(2 * ARRIVAL.index(k // per) * size + (k % per) * cap, cap)

    def slots_of(index):
        return pl.ds(pl.multiple_of(index * cap, cap), cap)

    def dispatch(k):
        peer = flipped(me, k)
        return pltpu.make_async_remote_copy(
            src_ref=slots.at[slots_of(peer)],
            dst_ref=rows.at[0, spot_of(k)],
            send_sem=disp_send.at[k],
            recv_sem=disp_recv.at[k],
            device_id={"sp": peer},
            device_id_type=MESH,
        )

    def giveback(k):
        peer = flipped(me, k)
        return pltpu.make_async_remote_copy(
            src_ref=outp.at[0, spot_of(k)],
            dst_ref=out.at[slots_of(me)],
            send_sem=ret_send.at[k],
            recv_sem=ret_recv.at[k],
            device_id={"sp": peer},
            device_id_type=MESH,
        )

    def hop(kind, g, source, target, other):
        return pltpu.make_async_remote_copy(
            src_ref=source,
            dst_ref=target,
            send_sem=hop_send.at[kind, g],
            recv_sem=hop_recv.at[kind, g],
            device_id={"tp": other},
            device_id_type=MESH,
        )

    def rows_near(g):
        return hop(0, g, rows.at[0, spot(g, 0)], rows.at[0, spot(g, 1)], near)

    def rows_far(g):
        return hop(1, g, rows.at[0, spot(g, 0)], rows.at[1, spot(g, 0)], far)

    def rows_far_near(g):
        return hop(2, g, rows.at[1, spot(g, 0)], rows.at[1, spot(g, 1)], near)

    def part_near(side, g):
        return hop(
            3 + side, g, outp.at[side, spot(g, 1)], nrecv.at[side, pl.ds(g * size, size)], near
        )

    def part_far(g):
        return hop(5, g, outp.at[1, spot(g, 0)], frecv.at[pl.ds(g * size, size)], far)

    kept = pltpu.make_async_copy(slots.at[slots_of(me)], rows.at[0, spot_of(0)], local_sem)
    kept.start()
    for g in ARRIVAL:
        for k in range(g * per, (g + 1) * per):
            if k:
                dispatch(k).start()

    def forward(g):
        for k in range(g * per, (g + 1) * per):
            if k:
                dispatch(k).wait_recv()
            else:
                kept.wait()
        rows_far(g).start()
        rows_near(g).start()

    def forward_far(g):
        rows_far(g).wait_recv()
        rows_far_near(g).start()

    def compute(side, pair):
        both = ARRIVAL[2 * pair : 2 * pair + 2]
        for g in both:
            (rows_far_near(g) if side else rows_near(g)).wait_recv()
        if side == 0 and pair == 0:
            loads[0].wait()
            loads[1].wait()
        tile = pl.ds(4 * pair * size, 4 * size)
        step = min(256, hidden)

        @pl.loop(0, hidden // step)
        def _(j):
            columns = pl.ds(pl.multiple_of(j * step, step), step)
            tokens = rows[side, tile, :]
            gate_pre = jnp.dot(tokens, gate[:, columns], preferred_element_type=jnp.float32)
            up_pre = jnp.dot(tokens, up[:, columns], preferred_element_type=jnp.float32)
            gated = jnp.minimum(gate_pre, LIMIT)
            upper = jnp.clip(up_pre, -LIMIT, LIMIT)
            act[:, columns] = (
                (upper + 1.0) * gated * jax.nn.sigmoid(SLOPE * gated)
            ).astype(jnp.bfloat16)

        if side == 0 and pair == 0:
            loads[2].wait()
        wide = 512

        @pl.loop(0, width // wide)
        def _(j):
            columns = pl.ds(pl.multiple_of(j * wide, wide), wide)
            outp[side, tile, columns] = jnp.dot(
                act[...], down[:, columns], preferred_element_type=jnp.float32
            ).astype(jnp.bfloat16)

        for g in both:
            part_near(side, g).start()

    def chip_sum(g):
        part_near(1, g).wait_recv()
        mine = outp[1, spot(g, 0), :].astype(jnp.float32)
        other = nrecv[1, pl.ds(g * size, size), :].astype(jnp.float32)
        outp[1, spot(g, 0), :] = (mine + other).astype(jnp.bfloat16)
        part_far(g).start()

    home = pltpu.make_async_copy(outp.at[0, spot_of(0)], out.at[slots_of(me)], local_sem)

    def finish(g):
        part_near(0, g).wait_recv()
        mine = outp[0, spot(g, 0), :].astype(jnp.float32)
        other = nrecv[0, pl.ds(g * size, size), :].astype(jnp.float32)
        part_far(g).wait_recv()
        distant = frecv[pl.ds(g * size, size), :].astype(jnp.float32)
        outp[0, spot(g, 0), :] = (mine + other + distant).astype(jnp.bfloat16)
        for k in range(g * per, (g + 1) * per):
            if k:
                giveback(k).start()
            else:
                home.start()

    o = ARRIVAL
    forward(o[0])
    forward(o[1])
    forward_far(o[0])
    compute(0, 0)
    forward(o[2])
    forward(o[3])
    forward_far(o[1])
    compute(1, 0)
    compute(0, 1)
    forward(o[4])
    forward_far(o[2])
    forward_far(o[3])
    compute(1, 1)
    forward(o[5])
    compute(0, 2)
    forward_far(o[4])
    forward(o[6])
    forward(o[7])
    chip_sum(4)
    forward_far(o[5])
    compute(1, 2)
    compute(0, 3)
    chip_sum(5)
    forward_far(o[6])
    forward_far(o[7])
    compute(1, 3)
    for g in RETURN:
        if g not in (4, 5):
            chip_sum(g)
    for g in RETURN:
        finish(g)
    for k in range(1, count):
        dispatch(k).wait_send()
    for g in range(GROUPS):
        rows_near(g).wait_send()
        rows_far(g).wait_send()
        rows_far_near(g).wait_send()
        part_near(0, g).wait_send()
        part_near(1, g).wait_send()
        part_far(g).wait_send()
    home.wait()
    for k in range(1, count):
        giveback(k).wait()


def run_experts(count, slots, gate_matrix, up_matrix, down_matrix):
    total, width = slots.shape
    hidden = down_matrix.shape[0]
    size = total // GROUPS
    dtype = slots.dtype
    anywhere = pl.BlockSpec(memory_space=pl.ANY)
    return pl.pallas_call(
        functools.partial(experts_kernel, count),
        out_shape=jax.ShapeDtypeStruct(slots.shape, dtype),
        in_specs=[anywhere] * 4,
        out_specs=anywhere,
        scratch_shapes=[
            pltpu.VMEM((2, 2 * total, width), dtype),
            pltpu.VMEM((2, 2 * total, width), dtype),
            pltpu.VMEM((2, total, width), dtype),
            pltpu.VMEM((total, width), dtype),
            pltpu.VMEM((4 * size, hidden), dtype),
            pltpu.VMEM((width, hidden), dtype),
            pltpu.VMEM((width, hidden), dtype),
            pltpu.VMEM((hidden, width), dtype),
            pltpu.SemaphoreType.DMA((3,)),
            pltpu.SemaphoreType.DMA,
            pltpu.SemaphoreType.DMA((count,)),
            pltpu.SemaphoreType.DMA((count,)),
            pltpu.SemaphoreType.DMA((6, GROUPS)),
            pltpu.SemaphoreType.DMA((6, GROUPS)),
            pltpu.SemaphoreType.DMA((count,)),
            pltpu.SemaphoreType.DMA((count,)),
        ],
        compiler_params=pltpu.CompilerParams(
            collective_id=0, has_side_effects=True, vmem_limit_bytes=60 * 2**20
        ),
        cost_estimate=pl.CostEstimate(
            flops=24 * total * width * hidden,
            bytes_accessed=10 * total * width,
            transcendentals=4 * total * hidden,
        ),
        name="experts",
    )(slots, gate_matrix, up_matrix, down_matrix)


def shards(
    glu_value,
    glu_gate,
    conv_kernel,
    norm_gain,
    mix_weight,
    residual,
    resid_gain,
    expert_ids,
    route_weight,
    w_gate,
    w_up,
    w_down,
    out_gain,
):
    gate_local, up_local, down_local = w_gate[0], w_up[0], w_down[0]
    gated_in = (
        glu_value.astype(jnp.float32) * jax.nn.sigmoid(glu_gate.astype(jnp.float32))
    ).astype(jnp.bfloat16)
    reach_back = conv_kernel.shape[0] - 1
    length = gated_in.shape[0]
    before_rows = shifted(gated_in[length - reach_back :], "sp", 1)
    extended = jnp.concatenate([before_rows, gated_in], axis=0).astype(jnp.float32)
    convolved = jnp.zeros(gated_in.shape, jnp.float32)
    for offset in range(reach_back + 1):
        convolved = convolved + conv_kernel[offset] * extended[offset : offset + length]
    channel_sum, squares = lax.psum(
        (jnp.sum(convolved, axis=1), jnp.sum(convolved * convolved, axis=1)), "tp"
    )
    centre = channel_sum / DC
    spread = squares / DC - centre * centre
    normed = (convolved - centre[:, None]) * lax.rsqrt(spread[:, None] + EPSILON) * norm_gain
    mix_in = jax.nn.silu(normed).astype(jnp.bfloat16)
    tp_count = lax.axis_size("tp")
    place = lax.axis_index("tp")
    own_count = length // tp_count
    width = residual.shape[1]
    products = jnp.dot(mix_in, mix_weight, preferred_element_type=jnp.float32)
    products = products.astype(jnp.bfloat16).reshape(tp_count // 2, 2, own_count, width)
    near = place % 2
    far = place // 2
    kept = lax.dynamic_index_in_dim(products, near, 1, False)
    given = lax.dynamic_index_in_dim(products, 1 - near, 1, False)
    pair_sum = kept.astype(jnp.float32) + swapped(given, 1).astype(jnp.float32)
    pair_kept = lax.dynamic_index_in_dim(pair_sum, far, 0, False)
    pair_given = lax.dynamic_index_in_dim(pair_sum, 1 - far, 0, False).astype(jnp.bfloat16)
    mixed_rows = pair_kept + swapped(pair_given, 2).astype(jnp.float32)
    hidden = normalize(residual.astype(jnp.float32) + mixed_rows, resid_gain).astype(jnp.bfloat16)
    experts = lax.axis_size("sp")
    top_count = expert_ids.shape[1]
    capacity = 2 * own_count * top_count // experts
    positions = slot_layout(expert_ids, experts, capacity)
    slots = jnp.arange(experts * capacity, dtype=jnp.int32)
    chosen = (positions[:, :, None] == slots).astype(jnp.float32)
    pick = jnp.sum(chosen, axis=1).astype(jnp.bfloat16)
    weights = jnp.sum(chosen * route_weight[:, :, None], axis=1)
    weights_high = weights.astype(jnp.bfloat16)
    weights_low = (weights - weights_high.astype(jnp.float32)).astype(jnp.bfloat16)
    dispatched = lax.dot_general(
        pick, hidden, (((0,), (0,)), ((), ())), preferred_element_type=jnp.float32
    ).astype(jnp.bfloat16)
    returned = run_experts(experts, dispatched, gate_local, up_local, down_local)
    routed_sum = jnp.dot(weights_high, returned, preferred_element_type=jnp.float32) + jnp.dot(
        weights_low, returned, preferred_element_type=jnp.float32
    )
    return normalize(hidden.astype(jnp.float32) + routed_sum, out_gain).astype(jnp.bfloat16)


def solution(mesh):
    in_specs = (
        P("sp", "tp"),
        P("sp", "tp"),
        P(None, "tp"),
        P("tp"),
        P("tp", None),
        P(("sp", "tp"), None),
        P(),
        P(("sp", "tp"), None),
        P(("sp", "tp"), None),
        P("sp", None, "tp"),
        P("sp", None, "tp"),
        P("sp", "tp", None),
        P(),
    )
    out_specs = P(("sp", "tp"), None)

    return jax.shard_map(shards, mesh=mesh, in_specs=in_specs, out_specs=out_specs, check_vma=False)
```

profile of v0, /device:TPU:0, one launch (start us, length us, event | category | flops | bytes accessed | tf_op | source)
XLA Modules:
  0.0 168.2 jit_solution(12556219341691584781)
XLA Ops:
  0.0 0.0 copy-start
  0.0 2.4 %multiply_convert_fusion.3 = bf16[512,512]{1,0:T(8,128)(2,1)} fusion(bf16[512,512]{1,0:T(8,128)(2,1)} %param.14, bf16[512,512]{1,0:T(8,128)(2,1)} %param.13), kind=kLoop, calls=%fused_computation.76 | loop fusion | flops 1835008 | bytes 1572864 | tf_op jit(solution)/shard_map/convert_element_type | solution.py:350
  2.4 0.8 slice.260
  3.2 4.9 %collective-permute-start = (bf16[30,512]{1,0:T(8,128)(2,1)S(1)}, bf16[30,512]{1,0:T(8,128)(2,1)S(1)}, u32[]{:S(2)}, u32[]{:S(2)}) collective-permute-start(bf16[30,512]{1,0:T(8,128)(2,1)S(1)} %slice.260), channel_id=1, source_target_pairs={{0,4},{4,8},{8,12},{12,16},{16,20},{20,24},{24,28},{1,5},{5,9},{9,... | collective-permute-start | bytes 92168 | tf_op jit(solution)/shard_map/ppermute | solution.py:21
  8.1 1.2 fusion.49
  9.3 1.0 fusion.50
  10.3 0.0 collective-permute-done
  10.3 1.2 maximum_convert_fusion
  11.5 0.0 copy-start.7
  11.6 5.8 %fusion.45 = (f32[512]{0:T(512)S(1)}, f32[512]{0:T(512)S(1)}, f32[512,512]{1,0:T(8,128)}) fusion(f32[542,512]{1,0:T(8,128)S(1)} %maximum_convert_fusion, f32[512]{0:T(512)S(1)} %bitcast.90, f32[512]{0:T(512)S(1)} %bitcast.91, f32[512]{0:T(512)S(1)} %bitcast.62, f32[512]{0:T(512)S(1)} %bitcast.63, f32[512]{0:T(512)S(1)} %bitcast.64, f32[512]{0:T(512)S(1)} %bitcast.65, ...), kind=kLoop, calls=%fused_computation.106 | loop fusion | flops 16776192 | bytes 33622016 | tf_op jit(solution)/shard_map/reduce_sum | solution.py:359
  17.4 6.5 %all-reduce = (f32[512]{0:T(512)S(1)}, f32[512]{0:T(512)S(1)}) all-reduce(f32[512]{0:T(512)S(1)} %get-tuple-element.6, f32[512]{0:T(512)S(1)} %get-tuple-element.5), channel_id=1, replica_groups=mesh['sp'=8,'tp'=4] {'tp'}, use_global_device_ids=true, to_apply=%region_3.0 | all-reduce | flops 1024 | bytes 8192 | tf_op jit(solution)/shard_map/psum | solution.py:358
  23.8 0.0 copy-done
  23.8 0.0 copy-done.7
  23.8 4.0 %convolution_convert_fusion.1 = bf16[512,2048]{1,0:T(8,128)(2,1)} fusion(bf16[512,2048]{1,0:T(8,128)(2,1)S(1)} %copy-done, f32[512,512]{1,0:T(8,128)} %get-tuple-element.13, f32[512]{0:T(512)S(1)} %copy-done.7, f32[512]{0:T(512)S(1)} %get-tuple-element.46, f32[512]{0:T(512)S(1)} %get-tuple-element.45), kind=kOutput, calls=%fused_computation.1 | convolution fusion | flops 1076887552 | bytes 5249024 | tf_op jit(solution)/shard_map/dot_general | solution.py:369
  27.9 0.0 copy-start.5
  27.9 2.3 %dynamic-slice_bitcast_fusion = bf16[2,128,2048]{2,1,0:T(8,128)(2,1)} fusion(bf16[2,2,128,2048]{3,2,1,0:T(8,128)(2,1)} %bitcast.31, s32[]{:T(128)S(6)} %select_n.27), kind=kLoop, calls=%fused_computation.73 | loop fusion | bytes 2097156 | tf_op jit(solution)/shard_map/jit(dynamic_index_in_dim)/squeeze | solution.py:374
  30.2 0.0 collective-permute-start.1
  30.2 0.0 copy-done.5
  30.2 0.1 copy.30
  30.3 0.1 eq.44
  30.5 0.1 eq.40
  30.6 0.6 reduce-window.6
  31.2 0.0 copy-start.6
  31.2 1.9 %collective-permute-done.1 = bf16[2,128,2048]{2,1,0:T(8,128)(2,1)S(1)} collective-permute-done((bf16[2,128,2048]{2,1,0:T(8,128)(2,1)}, bf16[2,128,2048]{2,1,0:T(8,128)(2,1)S(1)}, u32[]{:S(2)}, u32[]{:S(2)}) %collective-permute-start.1) | collective-permute-done | bytes 1048608 | tf_op jit(solution)/shard_map/ppermute | solution.py:32
  33.1 1.6 convert_add_fusion
  34.7 0.0 copy-start.2
  34.7 1.3 copy-done.2
  36.0 0.1 fusion.32
  36.1 1.2 collective-permute-start.2
  37.2 0.2 slice_reduce_fusion
  37.5 0.1 fusion.42
  37.6 0.1 reduce_sum.88
  37.7 0.1 copy.32
  37.8 0.0 copy-done.6
  37.8 0.2 select_reduce_fusion
  38.0 0.0 copy-start.3
  38.0 12.2 %collective-permute-done.2 = bf16[128,2048]{1,0:T(8,128)(2,1)} collective-permute-done((bf16[128,2048]{1,0:T(8,128)(2,1)S(1)}, bf16[128,2048]{1,0:T(8,128)(2,1)}, u32[]{:S(2)}, u32[]{:S(2)}) %collective-permute-start.2) | collective-permute-done | bytes 524320 | tf_op jit(solution)/shard_map/ppermute | solution.py:32
  50.2 1.8 %fusion.46 = (f32[128]{0:T(128)S(1)}, f32[128,2048]{1,0:T(8,128)S(1)}) fusion(bf16[128,2048]{1,0:T(8,128)(2,1)} %collective-permute-done.2, f32[2,128,2048]{2,1,0:T(8,128)} %copy-done.2, s32[]{:T(128)S(6)} %select_n.29, bf16[128,2048]{1,0:T(8,128)(2,1)} %param.18), kind=kLoop, calls=%fused_computation.107 | loop fusion | flops 1310592 | bytes 3146244 | tf_op jit(solution)/shard_map/reduce_sum | solution.py:25
  52.0 0.3 multiply_reduce_fusion.1
  52.3 0.0 copy-done.3
  52.3 2.2 %convolution_convert_fusion.slots = bf16[512,2048]{1,0:T(8,128)(2,1)} fusion(bf16[128,512]{1,0:T(8,128)(2,1)S(1)} %get-tuple-element.8, f32[128,2048]{1,0:T(8,128)S(1)} %get-tuple-element.12, f32[2048]{0:T(1024)S(1)} %copy-done.3, f32[128]{0:T(128)S(1)} %add_rsqrt_fusion.2, f32[128]{0:T(128)S(1)} %broadcast_multiply_fusion.2), kind=kOutput, calls=%fused_computation | convolution fusion | flops 270532608 | bytes 3286016 | tf_op jit(solution)/shard_map/dot_general | solution.py:390
  54.5 109.5 %experts.1 = bf16[512,2048]{1,0:T(8,128)(2,1)} custom-call(bf16[512,2048]{1,0:T(8,128)(2,1)} %convolution_convert_fusion.slots, bf16[2048,512]{1,0:T(8,128)(2,1)} %bitcast.92, bf16[2048,512]{1,0:T(8,128)(2,1)} %bitcast.93, bf16[512,2048]{1,0:T(8,128)(2,1)} %bitcast.94), custom_call_target="tpu_custom_call" | custom-call | flops 12884901888 | bytes 10485760 | tf_op jit(solution)/shard_map/experts/pallas_call | solution.py:297
  164.0 0.0 copy-start.1
  164.0 2.2 %fusion.39 = f32[128,2048]{1,0:T(8,128)S(1)} fusion(bf16[512,2048]{1,0:T(8,128)(2,1)} %experts.1, f32[128,512]{1,0:T(8,128)S(1)} %get-tuple-element.7), kind=kOutput, calls=%fused_computation.89 | convolution fusion | flops 268500992 | bytes 3407872 | tf_op jit(solution)/shard_map/dot_general | solution.py:394
  166.2 0.0 copy-done.1
  166.2 0.0 copy-start.4
  166.2 0.7 fusion.51
  166.9 0.3 multiply_reduce_fusion
  167.2 0.0 copy-done.4
  167.2 1.0 multiply_convert_fusion
  (9 shorter events, 0.1 us)
Async XLA Ops:
  0.0 23.8 %copy-start = (bf16[512,2048]{1,0:T(8,128)(2,1)S(1)}, bf16[512,2048]{1,0:T(8,128)(2,1)}, u32[]{:S(2)}) copy-start(bf16[512,2048]{1,0:T(8,128)(2,1)} %param.17) | copy-start | bytes 6291460
  3.2 7.1 %collective-permute-start = (bf16[30,512]{1,0:T(8,128)(2,1)S(1)}, bf16[30,512]{1,0:T(8,128)(2,1)S(1)}, u32[]{:S(2)}, u32[]{:S(2)}) collective-permute-start(bf16[30,512]{1,0:T(8,128)(2,1)S(1)} %slice.260), channel_id=1, source_target_pairs={{0,4},{4,8},{8,12},{12,16},{16,20},{20,24},{24,28},{1,5},{5,9},{9,... | collective-permute-start | bytes 92168 | tf_op jit(solution)/shard_map/ppermute | solution.py:21
  11.5 12.3 %copy-start.7 = (f32[512]{0:T(512)S(1)}, f32[512]{0:T(512)}, u32[]{:S(2)}) copy-start(f32[512]{0:T(512)} %param.16) | copy-start | bytes 6148
  27.9 2.3 %copy-start.5 = (s32[128,2]{0,1:T(2,128)S(1)}, s32[128,2]{0,1:T(2,128)}, u32[]{:S(2)}) copy-start(s32[128,2]{0,1:T(2,128)} %param.20) | copy-start | bytes 3076
  30.2 2.9 %collective-permute-start.1 = (bf16[2,128,2048]{2,1,0:T(8,128)(2,1)}, bf16[2,128,2048]{2,1,0:T(8,128)(2,1)S(1)}, u32[]{:S(2)}, u32[]{:S(2)}) collective-permute-start(bf16[2,128,2048]{2,1,0:T(8,128)(2,1)} %dynamic-slice_bitcast_fusion), channel_id=1, source_target_pairs={{0,1},{1,0},{2,3},{3,2},{4,5},{5,4},{6,7},{7,6},{8,9},{9,8},{10,11... | collective-permute-start | bytes 3145736 | tf_op jit(solution)/shard_map/ppermute | solution.py:32
  31.2 6.6 %copy-start.6 = (f32[128,2]{0,1:T(2,128)S(1)}, f32[128,2]{0,1:T(2,128)}, u32[]{:S(2)}) copy-start(f32[128,2]{0,1:T(2,128)} %param.21) | copy-start | bytes 3076
  34.7 1.4 copy-start.2
  36.1 14.1 %collective-permute-start.2 = (bf16[128,2048]{1,0:T(8,128)(2,1)S(1)}, bf16[128,2048]{1,0:T(8,128)(2,1)}, u32[]{:S(2)}, u32[]{:S(2)}) collective-permute-start(bf16[128,2048]{1,0:T(8,128)(2,1)S(1)} %fusion.32), channel_id=1, source_target_pairs={{0,2},{1,3},{2,0},{3,1},{4,6},{5,7},{6,4},{7,5},{8,10},{9,11},{10,... | collective-permute-start | bytes 1572872 | tf_op jit(solution)/shard_map/ppermute | solution.py:32
  38.0 14.3 %copy-start.3 = (f32[2048]{0:T(1024)S(1)}, f32[2048]{0:T(1024)}, u32[]{:S(2)}) copy-start(f32[2048]{0:T(1024)} %param.19) | copy-start | bytes 24580
  164.0 2.2 %copy-start.1 = (bf16[512,2048]{1,0:T(8,128)(2,1)S(1)}, bf16[512,2048]{1,0:T(8,128)(2,1)}, u32[]{:S(2)}) copy-start(bf16[512,2048]{1,0:T(8,128)(2,1)} %experts.1) | copy-start | bytes 6291460
  166.2 1.0 copy-start.4
where the time goes:
time: 169 us; the launch traced here: 168 us
  Pallas kernels  109 us (64%)
  other arithmetic  15.3 us (9%)
  waiting for transfers between devices  14.1 us (8%)
  matrix products  9.09 us (5%)
  local copies, waits for them, and re-layouts  7.54 us (4%)
  blocking collectives  6.45 us (4%)
  starting transfers between devices  6.06 us (4%)
    pallas_call x1, Pallas kernels, run_experts(): pl.pallas_call(functools.partial(experts_kernel, count), out_shape=jax.Sh...  109 us
    ppermute x2, waiting for transfers between devices, swapped(): return lax.ppermute(block, 'tp', route)  14.1 us
    psum x1, blocking collectives, shards(): lax.psum((jnp.sum(convolved, axis=1), jnp.sum(convolved * convolved, axis...  6.45 us
    reduce_sum x1, other arithmetic, shards(): jnp.sum(convolved, axis=1)  5.8 us
    ppermute x1, starting transfers between devices, shifted(): return lax.ppermute(block, axis, route)  4.9 us
    dot_general x1, matrix products, shards(): products = jnp.dot(mix_in, mix_weight, preferred_element_type=jnp.float32)  4.04 us
  transfers between devices with their start and end apart: 3, of which 2 were waited for; matrix products, arithmetic and copies ran while one was open for 2% of the time, Pallas kernels for 0%

commit v1 on v0

v1 whole, which is shorter than its diff:
```python
import functools

import jax
import jax.numpy as jnp
from jax import lax
from jax.experimental import pallas as pl
from jax.experimental.pallas import tpu as pltpu
from jax.sharding import PartitionSpec as P

EPSILON = 1e-05
LIMIT = 7.0
SLOPE = 1.702
HALO = 32
CHUNK = 64
PIECES = 4

MESH = pl.DeviceIdType.MESH
GROUPS = 8
ARRIVAL = (0, 1, 4, 2, 5, 3, 6, 7)
RETURN = (4, 5, 6, 7, 2, 3, 1, 0)


def flipped(index, mask):
    result = index
    bit = 1
    while bit <= mask:
        if mask & bit:
            result = result + bit - 2 * bit * lax.rem(lax.div(index, bit), 2)
        bit *= 2
    return result


def wide(values):
    return values.astype(jnp.float32)


def layer_kernel(
    count,
    places,
    value_hbm,
    glu_hbm,
    taps,
    norm_gain,
    mix_hbm,
    residual_hbm,
    resid_gain,
    ids,
    route,
    gate_hbm,
    up_hbm,
    down_hbm,
    out_gain,
    out,
    value,
    glu,
    mix,
    residual,
    gate,
    up,
    down,
    halo_out,
    halo_in,
    extended,
    convolved,
    stats,
    stats_in,
    mix_in,
    products,
    near_in,
    far_out,
    far_in,
    hidden,
    before,
    chosen,
    pick,
    weigh,
    high,
    low,
    slots,
    rows,
    outp,
    nrecv,
    frecv,
    act,
    returned,
    combined,
    load_sem,
    halo_send,
    halo_recv,
    stat_send,
    stat_recv,
    mixn_send,
    mixn_recv,
    mixf_send,
    mixf_recv,
    disp_send,
    disp_recv,
    hop_send,
    hop_recv,
    ret_send,
    ret_recv,
):
    me = lax.axis_index("sp")
    place = lax.axis_index("tp")
    near = flipped(place, 1)
    far = flipped(place, 2)
    across = flipped(place, 3)
    core = lax.rem(place, 2)
    side_x = lax.div(place, 2)

    length, channels = value.shape
    half = length // 2
    block = half // 2
    width = mix.shape[1]
    units = down.shape[0]
    total = slots.shape[0]
    cap = total // count
    size = total // GROUPS
    per = count // GROUPS
    piece = width // PIECES

    loads = [
        pltpu.make_async_copy(source, target, load_sem.at[i])
        for i, (source, target) in enumerate(
            (
                (value_hbm, value),
                (glu_hbm, glu),
                (mix_hbm, mix),
                (residual_hbm, residual),
                (gate_hbm, gate),
                (up_hbm, up),
                (down_hbm, down),
            )
        )
    ]
    for load in loads:
        load.start()

    following = lax.rem(me + 1, count)
    previous = lax.rem(me + count - 1, count)
    barrier = pltpu.get_barrier_semaphore()
    for k in range(1, count):
        pl.semaphore_signal(barrier, inc=1, device_id={"sp": flipped(me, k)}, device_id_type=MESH)
    for other in (near, far, across):
        pl.semaphore_signal(barrier, inc=1, device_id={"tp": other}, device_id_type=MESH)

    def gated(first, rows_at_once):
        span = pl.ds(first, rows_at_once)
        return (wide(value[span, :]) * jax.nn.sigmoid(wide(glu[span, :]))).astype(jnp.bfloat16)

    loads[0].wait()
    loads[1].wait()
    tail = gated(length - HALO, HALO)
    halo_out[...] = tail
    extended[pl.ds(length, HALO), :] = wide(tail)

    @pl.loop(0, length // CHUNK)
    def _(i):
        first = pl.multiple_of(i * CHUNK, CHUNK)
        extended[pl.ds(first + HALO, CHUNK), :] = wide(gated(first, CHUNK))

    pl.semaphore_wait(barrier, count + 2)
    halo = pltpu.make_async_remote_copy(
        src_ref=halo_out,
        dst_ref=halo_in,
        send_sem=halo_send,
        recv_sem=halo_recv,
        device_id={"sp": following},
        device_id_type=MESH,
    )

    @pl.when(me < count - 1)
    def _():
        halo.start()

    @pl.when(me > 0)
    def _():
        halo.wait_recv()
        extended[pl.ds(0, HALO), :] = wide(halo_in[...])

    @pl.when(me == 0)
    def _():
        extended[pl.ds(0, HALO), :] = jnp.zeros((HALO, channels), jnp.float32)

    lanes = lax.broadcasted_iota(jnp.int32, (8, 128), 1)
    origin = (half * (1 - side_x), half * side_x)

    def convolve(h):
        def step(i, carry):
            sums, squares = carry
            first = pl.multiple_of(origin[h] + i * CHUNK, CHUNK)
            row_sum = jnp.zeros((CHUNK, 128), jnp.float32)
            row_square = jnp.zeros((CHUNK, 128), jnp.float32)
            for c in range(channels // 128):
                columns = pl.ds(c * 128, 128)
                window = extended[pl.ds(first, CHUNK + HALO), columns]
                result = jnp.zeros((CHUNK, 128), jnp.float32)
                reach = taps.shape[0]
                lead = HALO - reach + 1
                for phase in range(8):
                    moved = window
                    if phase:
                        moved = pltpu.roll(window, CHUNK + HALO - phase, 0)
                    for k in range(reach):
                        if (k + lead) % 8 == phase:
                            start = (k + lead) // 8 * 8
                            result = result + taps[k : k + 1, columns] * moved[start : start + CHUNK]
                convolved[h, pl.ds(pl.multiple_of(i * CHUNK, CHUNK), CHUNK), columns] = result
                row_sum = row_sum + result
                row_square = row_square + result * result
            for r in range(CHUNK // 8):
                here = lanes == i * (CHUNK // 8) + r
                part = jnp.sum(row_sum[8 * r : 8 * r + 8], axis=1, keepdims=True)
                sums = jnp.where(here, part, sums)
                part = jnp.sum(row_square[8 * r : 8 * r + 8], axis=1, keepdims=True)
                squares = jnp.where(here, part, squares)
            return sums, squares

        zero = jnp.zeros((8, 128), jnp.float32)
        sums, squares = lax.fori_loop(0, half // CHUNK, step, (zero, zero))
        stats[h, 0] = sums
        stats[h, 1] = squares

    def stat_copy(h, j, other):
        theirs = 1 - h if j else h
        return pltpu.make_async_remote_copy(
            src_ref=stats.at[h],
            dst_ref=stats_in.at[theirs, j],
            send_sem=stat_send.at[h, j],
            recv_sem=stat_recv.at[theirs, j],
            device_id={"tp": other},
            device_id_type=MESH,
        )

    def stat_copies(h):
        return [stat_copy(h, j, other) for j, other in enumerate((near, far, across))]

    def normalized(h):
        stat_copies(h)[0].wait_recv()
        for copy in stat_copies(1 - h)[1:]:
            copy.wait_recv()
        both = stats[h] + stats_in[h, 0] + stats_in[h, 1] + stats_in[h, 2]
        centre = both[0] / (places * channels)
        scale = lax.rsqrt(both[1] / (places * channels) - centre * centre + EPSILON)

        @pl.loop(0, half // 16)
        def _(i):
            parts = []
            for r in range(2):
                here = lanes == 2 * i + r
                middle = jnp.sum(jnp.where(here, centre, 0.0), axis=1, keepdims=True)
                factor = jnp.sum(jnp.where(here, scale, 0.0), axis=1, keepdims=True)
                first = pl.multiple_of(i * 16 + r * 8, 8)
                normed = (convolved[h, pl.ds(first, 8), :] - middle) * factor * norm_gain[...]
                parts.append(jax.nn.silu(normed))
            span = pl.ds(pl.multiple_of(i * 16, 16), 16)
            mix_in[h, span, :] = jnp.concatenate(parts, axis=0).astype(jnp.bfloat16)

    kept_rows = pl.ds(pl.multiple_of(core * block, block), block)
    given_rows = pl.ds(pl.multiple_of((1 - core) * block, block), block)

    def mix_near(h, p):
        return pltpu.make_async_remote_copy(
            src_ref=products.at[h, p, given_rows],
            dst_ref=near_in.at[h, p],
            send_sem=mixn_send.at[h, p],
            recv_sem=mixn_recv.at[h, p],
            device_id={"tp": near},
            device_id_type=MESH,
        )

    def mix_far(p):
        return pltpu.make_async_remote_copy(
            src_ref=far_out.at[p],
            dst_ref=far_in.at[p],
            send_sem=mixf_send.at[p],
            recv_sem=mixf_recv.at[p],
            device_id={"tp": far},
            device_id_type=MESH,
        )

    def project(h):
        for p in range(PIECES):
            products[h, p] = jnp.dot(
                mix_in[h], mix[:, p * piece : (p + 1) * piece], preferred_element_type=jnp.float32
            ).astype(jnp.bfloat16)
            mix_near(h, p).start()

    convolve(0)
    for copy in stat_copies(0):
        copy.start()
    convolve(1)
    for copy in stat_copies(1):
        copy.start()

    experts = lax.broadcasted_iota(jnp.int32, (count, block), 0)
    named = [ids[j : j + 1, :] == experts for j in range(ids.shape[0])]
    hits = jnp.zeros((count, block), jnp.float32)
    shares = jnp.zeros((count, block), jnp.float32)
    for j, match in enumerate(named):
        hits = hits + jnp.where(match, 1.0, 0.0)
        shares = shares + jnp.where(match, route[j : j + 1, :], 0.0)
    earlier = lax.broadcasted_iota(jnp.int32, (block, block), 0)
    later = lax.broadcasted_iota(jnp.int32, (block, block), 1)
    triangle = jnp.where(earlier < later, 1.0, 0.0).astype(jnp.bfloat16)
    ranks = jnp.dot(hits.astype(jnp.bfloat16), triangle, preferred_element_type=jnp.float32)
    before[...] = jnp.where(hits > 0.0, ranks, -1.0)
    chosen[...] = shares
    rank = lax.broadcasted_iota(jnp.int32, (cap, block), 0).astype(jnp.float32)
    for k in range(count):
        expert = flipped(me, k)
        match = before[pl.ds(expert, 1), :] == rank
        pick[pl.ds(k * cap, cap), :] = jnp.where(match, 1.0, 0.0)
        weigh[pl.ds(k * cap, cap), :] = jnp.where(match, chosen[pl.ds(expert, 1), :], 0.0)
    turned = weigh[...].T
    upper_part = turned.astype(jnp.bfloat16)
    high[...] = upper_part
    low[...] = (turned - wide(upper_part)).astype(jnp.bfloat16)

    normalized(0)
    loads[2].wait()
    project(0)
    for p in range(PIECES):
        mix_near(0, p).wait_recv()
        far_out[p] = (wide(products[0, p, kept_rows, :]) + wide(near_in[0, p])).astype(jnp.bfloat16)
        mix_far(p).start()
    normalized(1)
    project(1)

    def normalize(values, gain):
        centred = values - jnp.mean(values, axis=1, keepdims=True)
        spread = jnp.mean(centred * centred, axis=1, keepdims=True)
        return centred * lax.rsqrt(spread + EPSILON) * gain

    loads[3].wait()
    for p in range(PIECES):
        mix_near(1, p).wait_recv()
    for p in range(PIECES):
        mix_far(p).wait_recv()

    @pl.loop(0, block // 16)
    def _(i):
        span = pl.ds(pl.multiple_of(i * 16, 16), 16)
        own = pl.ds(pl.multiple_of(core * block + i * 16, 16), 16)
        mixed = jnp.concatenate(
            [
                wide(products[1, p, own, :]) + wide(near_in[1, p, span, :]) + wide(far_in[p, span, :])
                for p in range(PIECES)
            ],
            axis=1,
        )
        hidden[span, :] = normalize(wide(residual[span, :]) + mixed, resid_gain[...]).astype(
            jnp.bfloat16
        )

    def spot(g, side):
        return pl.ds((2 * ARRIVAL.index(g) + side) * size, size)

    def spot_of(k):
        return pl.ds(2 * ARRIVAL.index(k // per) * size + (k % per) * cap, cap)

    def dispatch(k):
        return pltpu.make_async_remote_copy(
            src_ref=slots.at[pl.ds(k * cap, cap)],
            dst_ref=rows.at[0, spot_of(k)],
            send_sem=disp_send.at[k],
            recv_sem=disp_recv.at[k],
            device_id={"sp": flipped(me, k)},
            device_id_type=MESH,
        )

    def giveback(k):
        return pltpu.make_async_remote_copy(
            src_ref=outp.at[0, spot_of(k)],
            dst_ref=returned.at[pl.ds(k * cap, cap)],
            send_sem=ret_send.at[k],
            recv_sem=ret_recv.at[k],
            device_id={"sp": flipped(me, k)},
            device_id_type=MESH,
        )

    def hop(kind, g, source, target, other):
        return pltpu.make_async_remote_copy(
            src_ref=source,
            dst_ref=target,
            send_sem=hop_send.at[kind, g],
            recv_sem=hop_recv.at[kind, g],
            device_id={"tp": other},
            device_id_type=MESH,
        )

    def rows_near(g):
        return hop(0, g, rows.at[0, spot(g, 0)], rows.at[0, spot(g, 1)], near)

    def rows_far(g):
        return hop(1, g, rows.at[0, spot(g, 0)], rows.at[1, spot(g, 0)], far)

    def rows_far_near(g):
        return hop(2, g, rows.at[1, spot(g, 0)], rows.at[1, spot(g, 1)], near)

    def part_near(side, g):
        return hop(
            3 + side, g, outp.at[side, spot(g, 1)], nrecv.at[side, pl.ds(g * size, size)], near
        )

    def part_far(g):
        return hop(5, g, outp.at[1, spot(g, 0)], frecv.at[pl.ds(g * size, size)], far)

    def send_group(g):
        for k in range(g * per, (g + 1) * per):
            if k:
                dispatch(k).start()

    for index, g in enumerate(ARRIVAL):
        span = pl.ds(g * size, size)
        picked = jnp.dot(
            pick[span, :].astype(jnp.bfloat16), hidden[...], preferred_element_type=jnp.float32
        ).astype(jnp.bfloat16)
        slots[span, :] = picked
        if g == 0:
            rows[0, spot_of(0), :] = slots[pl.ds(0, cap), :]
        if index:
            send_group(ARRIVAL[index - 1])
    send_group(ARRIVAL[-1])

    def forward(g):
        for k in range(g * per, (g + 1) * per):
            if k:
                dispatch(k).wait_recv()
        rows_far(g).start()
        rows_near(g).start()

    def forward_far(g):
        rows_far(g).wait_recv()
        rows_far_near(g).start()

    def compute(side, pair):
        both = ARRIVAL[2 * pair : 2 * pair + 2]
        for g in both:
            (rows_far_near(g) if side else rows_near(g)).wait_recv()
        if side == 0 and pair == 0:
            loads[4].wait()
            loads[5].wait()
        tile = pl.ds(4 * pair * size, 4 * size)
        step = min(256, units)

        @pl.loop(0, units // step)
        def _(j):
            columns = pl.ds(pl.multiple_of(j * step, step), step)
            tokens = rows[side, tile, :]
            gate_pre = jnp.dot(tokens, gate[:, columns], preferred_element_type=jnp.float32)
            up_pre = jnp.dot(tokens, up[:, columns], preferred_element_type=jnp.float32)
            clipped = jnp.minimum(gate_pre, LIMIT)
            upper = jnp.clip(up_pre, -LIMIT, LIMIT)
            act[:, columns] = (
                (upper + 1.0) * clipped * jax.nn.sigmoid(SLOPE * clipped)
            ).astype(jnp.bfloat16)

        if side == 0 and pair == 0:
            loads[6].wait()

        @pl.loop(0, PIECES)
        def _(j):
            columns = pl.ds(pl.multiple_of(j * piece, piece), piece)
            outp[side, tile, columns] = jnp.dot(
                act[...], down[:, columns], preferred_element_type=jnp.float32
            ).astype(jnp.bfloat16)

        for g in both:
            part_near(side, g).start()

    def chip_sum(g):
        part_near(1, g).wait_recv()
        mine = wide(outp[1, spot(g, 0), :])
        other = wide(nrecv[1, pl.ds(g * size, size), :])
        outp[1, spot(g, 0), :] = (mine + other).astype(jnp.bfloat16)
        part_far(g).start()

    def finish(g):
        part_near(0, g).wait_recv()
        mine = wide(outp[0, spot(g, 0), :])
        other = wide(nrecv[0, pl.ds(g * size, size), :])
        part_far(g).wait_recv()
        distant = wide(frecv[pl.ds(g * size, size), :])
        outp[0, spot(g, 0), :] = (mine + other + distant).astype(jnp.bfloat16)
        for k in range(g * per, (g + 1) * per):
            if k:
                giveback(k).start()
            else:
                returned[pl.ds(0, cap), :] = outp[0, spot_of(0), :]

    o = ARRIVAL
    forward(o[0])
    forward(o[1])
    forward_far(o[0])
    compute(0, 0)
    forward(o[2])
    forward(o[3])
    forward_far(o[1])
    compute(1, 0)
    compute(0, 1)
    forward(o[4])
    forward_far(o[2])
    forward_far(o[3])
    compute(1, 1)
    forward(o[5])
    compute(0, 2)
    forward_far(o[4])
    forward(o[6])
    forward(o[7])
    chip_sum(4)
    forward_far(o[5])
    compute(1, 2)
    compute(0, 3)
    chip_sum(5)
    forward_far(o[6])
    forward_far(o[7])
    compute(1, 3)
    for g in RETURN:
        if g not in (4, 5):
            chip_sum(g)
    for g in RETURN:
        finish(g)

    for k in range(1, count):
        giveback(k).wait_recv()

    @pl.loop(0, PIECES)
    def _(j):
        columns = pl.ds(pl.multiple_of(j * piece, piece), piece)
        values = returned[:, columns]
        combined[:, columns] = jnp.dot(
            high[...], values, preferred_element_type=jnp.float32
        ) + jnp.dot(low[...], values, preferred_element_type=jnp.float32)

    @pl.loop(0, block // 16)
    def _(i):
        span = pl.ds(pl.multiple_of(i * 16, 16), 16)
        out[span, :] = normalize(
            wide(hidden[span, :]) + combined[span, :], out_gain[...]
        ).astype(jnp.bfloat16)

    @pl.when(me < count - 1)
    def _():
        halo.wait_send()

    for h in range(2):
        for copy in stat_copies(h):
            copy.wait_send()
        for p in range(PIECES):
            mix_near(h, p).wait_send()
    for p in range(PIECES):
        mix_far(p).wait_send()
    for k in range(1, count):
        dispatch(k).wait_send()
        giveback(k).wait_send()
    for g in range(GROUPS):
        rows_near(g).wait_send()
        rows_far(g).wait_send()
        rows_far_near(g).wait_send()
        part_near(0, g).wait_send()
        part_near(1, g).wait_send()
        part_far(g).wait_send()


def layer(
    glu_value,
    glu_gate,
    conv_kernel,
    norm_gain,
    mix_weight,
    residual,
    resid_gain,
    expert_ids,
    route_weight,
    w_gate,
    w_up,
    w_down,
    out_gain,
):
    count = lax.axis_size("sp")
    places = lax.axis_size("tp")
    length, channels = glu_value.shape
    block, width = residual.shape
    units = w_down.shape[1]
    top = expert_ids.shape[1]
    total = 2 * block * top
    size = total // GROUPS
    half = length // 2
    piece = width // PIECES
    low_type = glu_value.dtype
    anywhere = pl.BlockSpec(memory_space=pl.ANY)
    inside = pl.BlockSpec(memory_space=pltpu.VMEM)

    def vmem(*shape, dtype=low_type):
        return pltpu.VMEM(shape, dtype)

    def wide_vmem(*shape):
        return pltpu.VMEM(shape, jnp.float32)

    scratch = [
        vmem(length, channels),
        vmem(length, channels),
        vmem(channels, width),
        vmem(block, width),
        vmem(width, units),
        vmem(width, units),
        vmem(units, width),
        vmem(HALO, channels),
        vmem(HALO, channels),
        wide_vmem(length + HALO, channels),
        wide_vmem(2, half, channels),
        wide_vmem(2, 2, 8, 128),
        wide_vmem(2, places - 1, 2, 8, 128),
        vmem(2, half, channels),
        vmem(2, PIECES, half, piece),
        vmem(2, PIECES, block, piece),
        vmem(PIECES, block, piece),
        vmem(PIECES, block, piece),
        vmem(block, width),
        wide_vmem(count, block),
        wide_vmem(count, block),
        wide_vmem(total, block),
        wide_vmem(total, block),
        vmem(block, total),
        vmem(block, total),
        vmem(total, width),
        vmem(2, 2 * total, width),
        vmem(2, 2 * total, width),
        vmem(2, total, width),
        vmem(total, width),
        vmem(4 * size, units),
        vmem(total, width),
        wide_vmem(block, width),
        pltpu.SemaphoreType.DMA((7,)),
        pltpu.SemaphoreType.DMA,
        pltpu.SemaphoreType.DMA,
        pltpu.SemaphoreType.DMA((2, places - 1)),
        pltpu.SemaphoreType.DMA((2, places - 1)),
        pltpu.SemaphoreType.DMA((2, PIECES)),
        pltpu.SemaphoreType.DMA((2, PIECES)),
        pltpu.SemaphoreType.DMA((PIECES,)),
        pltpu.SemaphoreType.DMA((PIECES,)),
        pltpu.SemaphoreType.DMA((count,)),
        pltpu.SemaphoreType.DMA((count,)),
        pltpu.SemaphoreType.DMA((6, GROUPS)),
        pltpu.SemaphoreType.DMA((6, GROUPS)),
        pltpu.SemaphoreType.DMA((count,)),
        pltpu.SemaphoreType.DMA((count,)),
    ]
    return pl.pallas_call(
        functools.partial(layer_kernel, count, places),
        out_shape=jax.ShapeDtypeStruct((block, width), low_type),
        in_specs=[
            anywhere,
            anywhere,
            inside,
            inside,
            anywhere,
            anywhere,
            inside,
            inside,
            inside,
            anywhere,
            anywhere,
            anywhere,
            inside,
        ],
        out_specs=inside,
        scratch_shapes=scratch,
        compiler_params=pltpu.CompilerParams(
            collective_id=0, has_side_effects=True, vmem_limit_bytes=62 * 2**20
        ),
        cost_estimate=pl.CostEstimate(
            flops=24 * total * width * units,
            bytes_accessed=10 * total * width,
            transcendentals=4 * total * units,
        ),
        name="layer",
    )(
        glu_value,
        glu_gate,
        conv_kernel,
        norm_gain[None, :],
        mix_weight,
        residual,
        resid_gain[None, :],
        expert_ids.T,
        route_weight.T,
        w_gate[0],
        w_up[0],
        w_down[0],
        out_gain[None, :],
    )


def solution(mesh):
    in_specs = (
        P("sp", "tp"),
        P("sp", "tp"),
        P(None, "tp"),
        P("tp"),
        P("tp", None),
        P(("sp", "tp"), None),
        P(),
        P(("sp", "tp"), None),
        P(("sp", "tp"), None),
        P("sp", None, "tp"),
        P("sp", None, "tp"),
        P("sp", "tp", None),
        P(),
    )

    return jax.shard_map(
        layer,
        mesh=mesh,
        in_specs=in_specs,
        out_specs=P(("sp", "tp"), None),
        check_vma=False,
    )
```

time: 169 us -> 147 us (0.87)
  Pallas kernels: 109 us -> 143 us
  other arithmetic: 15.3 us -> 0 us
  waiting for transfers between devices: 14.1 us -> 0 us
  matrix products: 9.09 us -> 0 us
  blocking collectives: 6.45 us -> 0 us
  starting transfers between devices: 6.06 us -> 0 us
  local copies, waits for them, and re-layouts: 7.54 us -> 1.88 us
    pallas_call x1, Pallas kernels: 109 us -> 143 us  [layer(): pl.pallas_call(functools.partial(layer_kernel, count, places), out_shape=...]
    ppermute x3 -> x0, waiting for transfers between devices: 14.1 us -> none  [the longest x2 14.1 us: swapped(): return lax.ppermute(block, 'tp', route)]
    dot_general x4 -> x0, matrix products: 9.09 us -> none  [the longest x1 4.04 us: shards(): products = jnp.dot(mix_in, mix_weight, preferred_element_type=jnp.float32)]
    reduce_sum x6 -> x0, other arithmetic: 8.39 us -> none  [the longest x1 5.8 us: shards(): jnp.sum(convolved, axis=1)]
    psum x1 -> x0, blocking collectives: 6.45 us -> none  [shards(): lax.psum((jnp.sum(convolved, axis=1), jnp.sum(convolved * convolved, axis...]
    ppermute x3 -> x0, starting transfers between devices: 6.06 us -> none  [the longest x1 4.9 us: shifted(): return lax.ppermute(block, axis, route)]
    convert_element_type x4 -> x0, other arithmetic: 4.65 us -> none  [the longest x1 2.44 us: shards(): gated_in = (glu_value.astype(jnp.float32) * jax.nn.sigmoid(glu_gate.astyp...]
    slice x4 -> x0, local copies, waits for them, and re-layouts: 3.15 us -> none  [the longest x2 2.17 us: shards(): conv_kernel[offset] * extended[offset:offset + length]]
  transfers between devices with their start and end apart: 3 -> 0, of which waited for: 2 -> 0; matrix products, arithmetic and copies ran while one was open for 2% -> 0% of each run, Pallas kernels for 0% -> 0%
where the time goes in v1:
time: 147 us; the launch traced here: 145 us
  Pallas kernels  143 us (97%)
  local copies, waits for them, and re-layouts  1.88 us (1%)
    pallas_call x1, Pallas kernels, layer(): pl.pallas_call(functools.partial(layer_kernel, count, places), out_shape=...  143 us

profile of v1, /device:TPU:0, one launch (start us, length us, event | category | flops | bytes accessed | tf_op | source)
XLA Modules:
  0.0 144.7 jit_solution(8693711825513085327)
XLA Ops:
  0.0 142.9 %layer.1 = bf16[128,2048]{1,0:T(8,128)(2,1)} custom-call(bf16[512,512]{1,0:T(8,128)(2,1)} %value_hbm.1, bf16[512,512]{1,0:T(8,128)(2,1)} %glu_hbm.1, f32[31,512]{1,0:T(8,128)} %taps.1, f32[1,512]{1,0:T(1,128)} %bitcast.13, bf16[512,2048]{1,0:T(8,128)(2,1)} %mix_hbm.1, bf16[128,2048]{1,0:T(8,128)(2,1)} %residual_hbm.1, f32[1,2048]{1,0:T(1,128)} %bitcast.11, ...), custom_call_target="tpu_custom_call" | custom-call | flops 12884901888 | bytes 10485760 | tf_op jit(solution)/shard_map/layer/pallas_call | solution.py:651
  142.9 1.9 %copy.15 = bf16[128,2048]{1,0:T(8,128)(2,1)} copy(bf16[128,2048]{1,0:T(8,128)(2,1)} %layer.1) | data formatting | bytes 1048576

commit v2 on v1

--- a/solution.py
+++ b/solution.py
@@ -16,8 +16,7 @@
 
 MESH = pl.DeviceIdType.MESH
 GROUPS = 8
-ARRIVAL = (0, 1, 4, 2, 5, 3, 6, 7)
-RETURN = (4, 5, 6, 7, 2, 3, 1, 0)
+ARRIVAL = (0, 1, 2, 4, 3, 5, 6, 7)
 
 
 def flipped(index, mask):
@@ -133,7 +132,7 @@
             )
         )
     ]
-    for load in loads:
+    for load in loads[:2]:
         load.start()
 
     following = lax.rem(me + 1, count)
@@ -150,6 +149,8 @@
 
     loads[0].wait()
     loads[1].wait()
+    for load in loads[2:]:
+        load.start()
     tail = gated(length - HALO, HALO)
     halo_out[...] = tail
     extended[pl.ds(length, HALO), :] = wide(tail)
@@ -173,22 +174,14 @@
     def _():
         halo.start()
 
-    @pl.when(me > 0)
-    def _():
-        halo.wait_recv()
-        extended[pl.ds(0, HALO), :] = wide(halo_in[...])
-
-    @pl.when(me == 0)
-    def _():
-        extended[pl.ds(0, HALO), :] = jnp.zeros((HALO, channels), jnp.float32)
-
     lanes = lax.broadcasted_iota(jnp.int32, (8, 128), 1)
-    origin = (half * (1 - side_x), half * side_x)
+    upper_first = (1, 0)
+    turn = (1 - side_x, side_x)
 
     def convolve(h):
         def step(i, carry):
             sums, squares = carry
-            first = pl.multiple_of(origin[h] + i * CHUNK, CHUNK)
+            first = pl.multiple_of(h * half + i * CHUNK, CHUNK)
             row_sum = jnp.zeros((CHUNK, 128), jnp.float32)
             row_square = jnp.zeros((CHUNK, 128), jnp.float32)
             for c in range(channels // 128):
@@ -222,12 +215,11 @@
         stats[h, 1] = squares
 
     def stat_copy(h, j, other):
-        theirs = 1 - h if j else h
         return pltpu.make_async_remote_copy(
             src_ref=stats.at[h],
-            dst_ref=stats_in.at[theirs, j],
+            dst_ref=stats_in.at[h, j],
             send_sem=stat_send.at[h, j],
-            recv_sem=stat_recv.at[theirs, j],
+            recv_sem=stat_recv.at[h, j],
             device_id={"tp": other},
             device_id_type=MESH,
         )
@@ -235,9 +227,9 @@
     def stat_copies(h):
         return [stat_copy(h, j, other) for j, other in enumerate((near, far, across))]
 
-    def normalized(h):
-        stat_copies(h)[0].wait_recv()
-        for copy in stat_copies(1 - h)[1:]:
+    def normalized(order):
+        h = turn[order]
+        for copy in stat_copies(h):
             copy.wait_recv()
         both = stats[h] + stats_in[h, 0] + stats_in[h, 1] + stats_in[h, 2]
         centre = both[0] / (places * channels)
@@ -254,7 +246,7 @@
                 normed = (convolved[h, pl.ds(first, 8), :] - middle) * factor * norm_gain[...]
                 parts.append(jax.nn.silu(normed))
             span = pl.ds(pl.multiple_of(i * 16, 16), 16)
-            mix_in[h, span, :] = jnp.concatenate(parts, axis=0).astype(jnp.bfloat16)
+            mix_in[order, span, :] = jnp.concatenate(parts, axis=0).astype(jnp.bfloat16)
 
     kept_rows = pl.ds(pl.multiple_of(core * block, block), block)
     given_rows = pl.ds(pl.multiple_of((1 - core) * block, block), block)
@@ -286,12 +278,19 @@
             ).astype(jnp.bfloat16)
             mix_near(h, p).start()
 
-    convolve(0)
-    for copy in stat_copies(0):
-        copy.start()
-    convolve(1)
-    for copy in stat_copies(1):
-        copy.start()
+    for h in upper_first:
+        if h == 0:
+            @pl.when(me > 0)
+            def _():
+                halo.wait_recv()
+                extended[pl.ds(0, HALO), :] = wide(halo_in[...])
+
+            @pl.when(me == 0)
+            def _():
+                extended[pl.ds(0, HALO), :] = jnp.zeros((HALO, channels), jnp.float32)
+        convolve(h)
+        for copy in stat_copies(h):
+            copy.start()
 
     experts = lax.broadcasted_iota(jnp.int32, (count, block), 0)
     named = [ids[j : j + 1, :] == experts for j in range(ids.shape[0])]
@@ -335,21 +334,18 @@
     loads[3].wait()
     for p in range(PIECES):
         mix_near(1, p).wait_recv()
+        columns = pl.ds(p * piece, piece)
+        combined[:, columns] = (
+            wide(residual[:, columns]) + wide(products[1, p, kept_rows, :]) + wide(near_in[1, p])
+        )
     for p in range(PIECES):
         mix_far(p).wait_recv()
 
-    @pl.loop(0, block // 16)
+    @pl.loop(0, block // 32)
     def _(i):
-        span = pl.ds(pl.multiple_of(i * 16, 16), 16)
-        own = pl.ds(pl.multiple_of(core * block + i * 16, 16), 16)
-        mixed = jnp.concatenate(
-            [
-                wide(products[1, p, own, :]) + wide(near_in[1, p, span, :]) + wide(far_in[p, span, :])
-                for p in range(PIECES)
-            ],
-            axis=1,
-        )
-        hidden[span, :] = normalize(wide(residual[span, :]) + mixed, resid_gain[...]).astype(
+        span = pl.ds(pl.multiple_of(i * 32, 32), 32)
+        distant = jnp.concatenate([wide(far_in[p, span, :]) for p in range(PIECES)], axis=1)
+        hidden[span, :] = normalize(combined[span, :] + distant, resid_gain[...]).astype(
             jnp.bfloat16
         )
 
@@ -406,10 +402,19 @@
     def part_far(g):
         return hop(5, g, outp.at[1, spot(g, 0)], frecv.at[pl.ds(g * size, size)], far)
 
+    def forward(g):
+        for k in range(g * per, (g + 1) * per):
+            if k:
+                dispatch(k).wait_recv()
+        rows_far(g).start()
+        rows_near(g).start()
+
     def send_group(g):
         for k in range(g * per, (g + 1) * per):
             if k:
                 dispatch(k).start()
+        if g == 0 and per == 1:
+            forward(g)
 
     for index, g in enumerate(ARRIVAL):
         span = pl.ds(g * size, size)
@@ -422,26 +427,21 @@
         if index:
             send_group(ARRIVAL[index - 1])
     send_group(ARRIVAL[-1])
-
-    def forward(g):
-        for k in range(g * per, (g + 1) * per):
-            if k:
-                dispatch(k).wait_recv()
-        rows_far(g).start()
-        rows_near(g).start()
+    if per > 1:
+        forward(0)
 
     def forward_far(g):
         rows_far(g).wait_recv()
         rows_far_near(g).start()
 
-    def compute(side, pair):
-        both = ARRIVAL[2 * pair : 2 * pair + 2]
+    def compute(side, *both):
         for g in both:
             (rows_far_near(g) if side else rows_near(g)).wait_recv()
-        if side == 0 and pair == 0:
+        if side == 0 and 0 in both:
             loads[4].wait()
             loads[5].wait()
-        tile = pl.ds(4 * pair * size, 4 * size)
+        count_rows = 2 * size * len(both)
+        tile = pl.ds(2 * ARRIVAL.index(both[0]) * size, count_rows)
         step = min(256, units)
 
         @pl.loop(0, units // step)
@@ -452,18 +452,18 @@
             up_pre = jnp.dot(tokens, up[:, columns], preferred_element_type=jnp.float32)
             clipped = jnp.minimum(gate_pre, LIMIT)
             upper = jnp.clip(up_pre, -LIMIT, LIMIT)
-            act[:, columns] = (
+            act[:count_rows, columns] = (
                 (upper + 1.0) * clipped * jax.nn.sigmoid(SLOPE * clipped)
             ).astype(jnp.bfloat16)
 
-        if side == 0 and pair == 0:
+        if side == 0 and 0 in both:
             loads[6].wait()
 
         @pl.loop(0, PIECES)
         def _(j):
             columns = pl.ds(pl.multiple_of(j * piece, piece), piece)
             outp[side, tile, columns] = jnp.dot(
-                act[...], down[:, columns], preferred_element_type=jnp.float32
+                act[:count_rows, :], down[:, columns], preferred_element_type=jnp.float32
             ).astype(jnp.bfloat16)
 
         for g in both:
@@ -489,56 +489,68 @@
             else:
                 returned[pl.ds(0, cap), :] = outp[0, spot_of(0), :]
 
-    o = ARRIVAL
-    forward(o[0])
-    forward(o[1])
-    forward_far(o[0])
-    compute(0, 0)
-    forward(o[2])
-    forward(o[3])
-    forward_far(o[1])
-    compute(1, 0)
-    compute(0, 1)
-    forward(o[4])
-    forward_far(o[2])
-    forward_far(o[3])
-    compute(1, 1)
-    forward(o[5])
-    compute(0, 2)
-    forward_far(o[4])
-    forward(o[6])
-    forward(o[7])
+    def combine(pair):
+        for k in range(2 * pair * per, 2 * (pair + 1) * per):
+            if k:
+                giveback(k).wait_recv()
+        inner = slice(2 * pair * size, 2 * (pair + 1) * size)
+        for p in range(PIECES):
+            columns = slice(p * piece, (p + 1) * piece)
+            values = returned[inner, columns]
+            combined[:, columns] += jnp.dot(
+                high[:, inner], values, preferred_element_type=jnp.float32
+            ) + jnp.dot(low[:, inner], values, preferred_element_type=jnp.float32)
+
+    forward(1)
+    forward_far(0)
+    compute(0, 0, 1)
+    forward(2)
+    forward(4)
+    forward_far(1)
+    compute(1, 0, 1)
+    compute(0, 2, 4)
+    forward(3)
+    forward_far(2)
+    forward_far(4)
+    compute(1, 2, 4)
+    forward(5)
     chip_sum(4)
-    forward_far(o[5])
-    compute(1, 2)
-    compute(0, 3)
+    compute(0, 3, 5)
+    forward_far(3)
+    forward(6)
+    forward_far(5)
+    compute(1, 3, 5)
+    forward(7)
     chip_sum(5)
-    forward_far(o[6])
-    forward_far(o[7])
-    compute(1, 3)
-    for g in RETURN:
-        if g not in (4, 5):
-            chip_sum(g)
-    for g in RETURN:
-        finish(g)
-
-    for k in range(1, count):
-        giveback(k).wait_recv()
-
-    @pl.loop(0, PIECES)
-    def _(j):
-        columns = pl.ds(pl.multiple_of(j * piece, piece), piece)
-        values = returned[:, columns]
-        combined[:, columns] = jnp.dot(
-            high[...], values, preferred_element_type=jnp.float32
-        ) + jnp.dot(low[...], values, preferred_element_type=jnp.float32)
-
-    @pl.loop(0, block // 16)
+    chip_sum(2)
+    compute(0, 6, 7)
+    finish(4)
+    forward_far(6)
+    compute(1, 6)
+    finish(5)
+    chip_sum(6)
+    forward_far(7)
+    compute(1, 7)
+    chip_sum(7)
+    chip_sum(3)
+    chip_sum(1)
+    chip_sum(0)
+    combined[...] = wide(hidden[...])
+    finish(2)
+    finish(6)
+    finish(7)
+    finish(3)
+    combine(2)
+    finish(1)
+    combine(3)
+    finish(0)
+    combine(1)
+    combine(0)
+
+    @pl.loop(0, block // 32)
     def _(i):
-        span = pl.ds(pl.multiple_of(i * 16, 16), 16)
-        out[span, :] = normalize(
-            wide(hidden[span, :]) + combined[span, :], out_gain[...]
-        ).astype(jnp.bfloat16)
+        span = pl.ds(pl.multiple_of(i * 32, 32), 32)
+        out[span, :] = normalize(combined[span, :], out_gain[...]).astype(jnp.bfloat16)
 
     @pl.when(me < count - 1)
     def _():

time: 147 us -> 140 us (0.952); the launches traced: 145 us -> 139 us
  Pallas kernels: 143 us -> 137 us
    pallas_call x1, Pallas kernels: 143 us -> 137 us  [layer(): pl.pallas_call(functools.partial(layer_kernel, count, places), out_shape=...]
where the time goes in v2:
time: 140 us; the launch traced here: 139 us
  Pallas kernels  137 us (98%)
  local copies, waits for them, and re-layouts  1.88 us (1%)
    pallas_call x1, Pallas kernels, layer(): pl.pallas_call(functools.partial(layer_kernel, count, places), out_shape=...  137 us

profile of v2, /device:TPU:0, one launch (start us, length us, event | category | flops | bytes accessed | tf_op | source)
XLA Modules:
  0.0 139.3 jit_solution(14129758417783727893)
XLA Ops:
  0.0 137.4 %layer.1 = bf16[128,2048]{1,0:T(8,128)(2,1)} custom-call(bf16[512,512]{1,0:T(8,128)(2,1)} %value_hbm.1, bf16[512,512]{1,0:T(8,128)(2,1)} %glu_hbm.1, f32[31,512]{1,0:T(8,128)} %taps.1, f32[1,512]{1,0:T(1,128)} %bitcast.13, bf16[512,2048]{1,0:T(8,128)(2,1)} %mix_hbm.1, bf16[128,2048]{1,0:T(8,128)(2,1)} %residual_hbm.1, f32[1,2048]{1,0:T(1,128)} %bitcast.11, ...), custom_call_target="tpu_custom_call" | custom-call | flops 12884901888 | bytes 10485760 | tf_op jit(solution)/shard_map/layer/pallas_call | solution.py:663
  137.4 1.9 %copy.15 = bf16[128,2048]{1,0:T(8,128)(2,1)} copy(bf16[128,2048]{1,0:T(8,128)(2,1)} %layer.1) | data formatting | bytes 1048576
